TPU v7x, 32 devices: a whole 2x2x4 slice. The times are simulated.
32 devices in a mesh: kv: 8 (over z, y), tp: 4 (over x, core).
Axes of the slice: x: 2, y: 2, z: 4, core: 2. Of those that a mesh axis runs over, the one named last changes fastest.
Arguments:
- inputs: bfloat16 [256, 4096], P(None, 'kv'), may hold values from -150 to 150
- norm_gain: bfloat16 [4096], P('kv'), may hold values from 0.099609375 to 1.8984375
- w_query: bfloat16 [4096, 2048], P('kv', 'tp'), may hold values from -0.09375 to 0.09375
- w_forget: bfloat16 [4096, 2048], P('kv', 'tp'), may hold values from -0.09375 to 0.09375
- w_value: bfloat16 [4096, 2048], P('kv', 'tp'), may hold values from -0.09375 to 0.09375
- lower_bound: float32 [2048], P('tp'), may hold values from 0.05 to 0.9
- head_gain: float32 [2048], P('tp'), may hold values from 0.1 to 1.9
- w_out: bfloat16 [2048, 4096], P('tp', 'kv'), may hold values from -0.125 to 0.125
- prior_state: float32 [64, 16, 128, 128], P('kv', 'tp'), may hold values from -3 to 3
- prev_forget: float32 [64, 4, 2048], P('kv', None, 'tp'), may hold values from 0.3 to 0.97
- prev_values: bfloat16 [64, 4, 2048], P('kv', None, 'tp'), may hold values from -6 to 6
- accepted: int32 [64], P('kv'), may hold values from 0 to 4
Outputs:
- mixed_out: bfloat16 [256, 4096], P(None, ('kv', 'tp'))
- base_state: float32 [64, 16, 128, 128], P('kv', 'tp')
All inputs are finite; a program needn't handle non-finite values.
Results may differ from a plain program's by a relative error of at most 0.01.
Values may be sent and summed in bfloat16 or wider, within the bound.
A program may use at most 64 MiB of HBM per device.

v0:
```python
import jax
import jax.numpy as jnp
from jax import lax
from jax.sharding import PartitionSpec as P

D = 4096


EPSILON = 1e-06


def recurrence(
    query_pre,
    forget_pre,
    value_pre,
    lower_bound,
    head_gain,
    prior_state,
    prev_forget,
    prev_values,
    accepted,
):
    sequences = prior_state.shape[0]
    heads = prior_state.shape[1]
    head_size = prior_state.shape[2]
    proposals = prev_forget.shape[1]
    layout = (sequences, proposals, heads, head_size)
    floor_gate = lower_bound.reshape(heads, head_size)
    forget_gate = floor_gate + (1.0 - floor_gate) * jax.nn.sigmoid(forget_pre.reshape(layout))
    keys_new = 1.0 - forget_gate
    queries = jax.nn.silu(query_pre.reshape(layout))
    values = value_pre.reshape(layout)
    old_gate = prev_forget.reshape(layout)
    old_values = prev_values.astype(jnp.float32).reshape(layout)
    carried = prior_state
    for position in range(proposals):
        folded = (
            old_gate[:, position, :, :, None] * carried
            + (1.0 - old_gate[:, position])[..., None] * old_values[:, position, :, None, :]
        )
        taken_up = (position < accepted)[:, None, None, None]
        carried = jnp.where(taken_up, folded, carried)
    base_state = carried
    results = []
    for position in range(proposals):
        carried = (
            forget_gate[:, position, :, :, None] * carried
            + keys_new[:, position, :, :, None] * values[:, position, :, None, :]
        )
        results.append(
            jnp.einsum(
                "shk,shkv->shv", queries[:, position], carried, precision=lax.Precision.HIGHEST
            )
        )
    stacked = jnp.stack(results, axis=1)
    inverse_rms = lax.rsqrt(jnp.mean(stacked * stacked, axis=-1, keepdims=True) + EPSILON)
    normed = stacked * inverse_rms * head_gain.reshape(heads, head_size)
    return (
        normed.astype(jnp.bfloat16).reshape(sequences * proposals, heads * head_size),
        base_state,
    )


def body(
    inputs,
    norm_gain,
    w_query,
    w_forget,
    w_value,
    lower_bound,
    head_gain,
    w_out,
    prior_state,
    prev_forget,
    prev_values,
    accepted,
):
    head_cols = w_query.shape[1]
    stacked_weight = jnp.concatenate((w_query, w_forget, w_value), axis=1)
    widened = inputs.astype(jnp.float32)
    scaled = (widened * norm_gain.astype(jnp.float32)).astype(jnp.bfloat16)
    local_squares = jnp.sum(widened * widened, axis=1)
    terms = jnp.dot(scaled, stacked_weight, preferred_element_type=jnp.float32)
    projected, squares = (
        lax.psum_scatter(terms, "kv", scatter_dimension=0, tiled=True),
        lax.psum_scatter(local_squares, "kv", scatter_dimension=0, tiled=True),
    )
    rscale = lax.rsqrt(squares / D + EPSILON)[:, None]
    query_pre = projected[:, :head_cols] * rscale
    forget_pre = projected[:, head_cols : 2 * head_cols] * rscale
    value_pre = projected[:, 2 * head_cols :] * rscale
    normed, base_state = recurrence(
        query_pre,
        forget_pre,
        value_pre,
        lower_bound,
        head_gain,
        prior_state,
        prev_forget,
        prev_values,
        accepted,
    )
    partial_value = jnp.dot(
        lax.all_gather(normed, "kv", axis=0, tiled=True), w_out, preferred_element_type=jnp.float32
    )
    mixed_out = lax.psum_scatter(
        partial_value.astype(jnp.bfloat16), "tp", scatter_dimension=1, tiled=True
    )
    return (mixed_out, base_state)


def solution(mesh):
    in_specs = (
        P(None, "kv"),
        P("kv"),
        P("kv", "tp"),
        P("kv", "tp"),
        P("kv", "tp"),
        P("tp"),
        P("tp"),
        P("tp", "kv"),
        P("kv", "tp", None, None),
        P("kv", None, "tp"),
        P("kv", None, "tp"),
        P("kv"),
    )
    out_specs = (P(None, ("kv", "tp")), P("kv", "tp", None, None))
    return jax.shard_map(body, mesh=mesh, in_specs=in_specs, out_specs=out_specs, check_vma=False)
```

profile of v0, /device:TPU:0, one launch (start us, length us, event | category | flops | bytes accessed | tf_op | source)
XLA Modules:
  0.0 160.9 jit_solution(14386743982602677634)
XLA Ops:
  7.2 0.0 reduce-scatter.5.cloned.1.call-start
  7.2 0.7 convert_element_type.18
  8.0 3.2 %fusion.6 = f32[256,1536]{1,0:T(8,128)} fusion(bf16[512,512]{1,0:T(8,128)(2,1)} %param.16, bf16[512,512]{1,0:T(8,128)(2,1)} %param.15, bf16[512,512]{1,0:T(8,128)(2,1)} %param.14, bf16[256,512]{1,0:T(8,128)(2,1)} %param.12, f32[512]{0:T(512)S(1)} %convert_element_type.18), kind=kOutput, calls=%fused_computation.10 | convolution fusion | flops 407764992 | bytes 3409920 | tf_op jit(solution)/shard_map/dot_general | solution.py:83
  11.2 0.0 reduce-scatter.5.cloned.1.call-update
  11.2 0.0 reduce-scatter.7.cloned.1.call-start
  11.3 0.6 dynamic-slice
  12.6 0.1 fusion.25
  12.8 23.3 %all-reduce = f32[256]{0:T(256)S(1)} all-reduce(f32[256]{0:T(256)S(1)} %fusion.25), channel_id=3, replica_groups=mesh['kv'=8,'tp'=4] {'kv'}, use_global_device_ids=true, to_apply=%region_2.0.clone | all-reduce | flops 256 | bytes 2048
  36.0 0.1 fusion.35
  36.2 7.0 %add_select_fusion = f32[8,4,128,128]{3,2,1,0:T(8,128)S(1)} fusion(f32[8,4,128,128]{3,2,1,0:T(8,128)} %param.20, f32[8,4,128]{2,1,0:T(4,128)S(1)} %get-tuple-element.34, f32[8,4,128]{2,1,0:T(4,128)S(1)} %get-tuple-element.30, f32[8,4,128]{2,1,0:T(4,128)S(1)} %get-tuple-element.32, f32[8,4,128]{2,1,0:T(4,128)S(1)} %get-tuple-element.29, ...), kind=kLoop, calls=%fused_computation.7 | loop fusion | flops 8388608 | bytes 4390944 | tf_op jit(solution)/shard_map/jit(_where)/select_n | solution.py:42
  43.2 36.6 %reduce-scatter.5.cloned.1.call-done = f32[32,1536]{1,0:T(8,128)} async-done(((f32[256,1536]{1,0:T(8,128)}), f32[32,1536]{1,0:T(8,128)}) %reduce-scatter.5.cloned.1.call-update) | async-done | bytes 196624 | tf_op jit(solution)/shard_map/reduce_scatter | solution.py:85
  79.9 1.0 fusion.33
  81.1 2.8 %fusion.4 = f32[8,4,1,128]{3,2,1,0:T(1,128)S(1)} fusion(f32[8,4,128,1]{2,3,1,0:T(1,128)S(1)} %bitcast.113, f32[8,4,128,128]{3,2,1,0:T(8,128)S(1)} %add_select_fusion, f32[8,4,128]{2,1,0:T(4,128)S(1)} %get-tuple-element.19, f32[8,4,128]{2,1,0:T(4,128)S(1)} %get-tuple-element.15, f32[8,4,128]{2,1,0:T(4,128)S(1)} %get-tuple-element.42), kind=kOutput, calls=%fused_computation.8 | convolution fusion | flops 7864320 | bytes 2179072 | tf_op jit(solution)/shard_map/shk,shkv->shv/dot_general | solution.py:51
  83.9 4.3 %fusion.26 = f32[8,4,1,128]{3,2,1,0:T(1,128)S(1)} fusion(f32[8,4,128,1]{2,3,1,0:T(1,128)S(1)} %bitcast.123, f32[8,4,128,128]{3,2,1,0:T(8,128)S(1)} %add_select_fusion, f32[8,4,128]{2,1,0:T(4,128)S(1)} %get-tuple-element.22, f32[8,4,128]{2,1,0:T(4,128)S(1)} %get-tuple-element.18, f32[8,4,128]{2,1,0:T(4,128)S(1)} %get-tuple-element.40, ...), kind=kOutput, calls=%fused_computation.33 | convolution fusion | flops 9437184 | bytes 2228224 | tf_op jit(solution)/shard_map/shk,shkv->shv/dot_general | solution.py:51
  88.2 6.1 %fusion.5 = f32[8,4,1,128]{3,2,1,0:T(1,128)S(1)} fusion(f32[8,4,128,1]{2,3,1,0:T(1,128)S(1)} %bitcast.122, f32[8,4,128]{2,1,0:T(4,128)S(1)} %get-tuple-element.21, f32[8,4,128]{2,1,0:T(4,128)S(1)} %get-tuple-element.17, f32[8,4,128]{2,1,0:T(4,128)S(1)} %get-tuple-element.41, f32[8,4,128,128]{3,2,1,0:T(8,128)S(1)} %add_select_fusion, ...), kind=kOutput, calls=%fused_computation.9 | convolution fusion | flops 11010048 | bytes 2277376 | tf_op jit(solution)/shard_map/shk,shkv->shv/dot_general | solution.py:51
  94.3 7.2 %fusion = f32[8,4,1,128]{3,2,1,0:T(1,128)S(1)} fusion(f32[8,4,128,1]{2,3,1,0:T(1,128)S(1)} %bitcast.121, f32[8,4,128]{2,1,0:T(4,128)S(1)} %get-tuple-element.20, f32[8,4,128]{2,1,0:T(4,128)S(1)} %get-tuple-element.16, f32[8,4,128]{2,1,0:T(4,128)S(1)} %get-tuple-element.39, f32[8,4,128]{2,1,0:T(4,128)S(1)} %get-tuple-element.21, ...), kind=kOutput, calls=%fused_computation | convolution fusion | flops 12582912 | bytes 2326528 | tf_op jit(solution)/shard_map/shk,shkv->shv/dot_general | solution.py:51
  101.5 0.1 multiply_reduce_fusion
  101.6 0.1 broadcast_multiply_fusion
  101.8 30.7 %all_gather.3 = bf16[256,512]{1,0:T(8,128)(2,1)S(1)} all-gather(bf16[32,512]{1,0:T(8,128)(2,1)S(1)} %fusion.29), channel_id=1, replica_groups=mesh['kv'=8,'tp'=4] {'kv'}, dimensions={0}, use_global_device_ids=true | all-gather | bytes 294912 | tf_op jit(solution)/shard_map/all_gather | solution.py:104
  132.5 0.3 convolution_convert_fusion
  132.8 0.8 copy.46
  133.7 0.0 reduce-scatter.7.cloned.1.call-update
  133.7 18.8 %reduce-scatter.7.cloned.1.call-done = bf16[128,256]{1,0:T(8,128)(2,1)} async-done(((bf16[512,256]{1,0:T(8,128)(2,1)}), bf16[128,256]{1,0:T(8,128)(2,1)}) %reduce-scatter.7.cloned.1.call-update) | async-done | bytes 65552
  152.4 1.6 copy.47
  (34 shorter events, 0.4 us)
Async XLA Ops:
  7.2 125.3 %copy-start = (bf16[512,512]{1,0:T(8,128)(2,1)S(1)}, bf16[512,512]{1,0:T(8,128)(2,1)}, u32[]{:S(2)}) copy-start(bf16[512,512]{1,0:T(8,128)(2,1)} %param.19) | copy-start | bytes 1572868
  7.2 72.7 %reduce-scatter.5.cloned.1.call-start = ((), (), s32[]{:S(2)}) async-start(), calls=%async_computation.2 | async-start | bytes 1769472 | tf_op jit(solution)/shard_map/reduce_scatter | solution.py:85
  8.0 3.3 %copy-start.8 = (u32[32]{0:T(128)S(1)}, u32[32]{0:T(128)}, u32[]{:S(2)}) copy-start(u32[32]{0:T(128)} %constant.27) | copy-start | bytes 388
  8.0 4.6 %copy-start.3 = (f32[8,4,512]{2,1,0:T(4,128)S(1)}, f32[8,4,512]{2,1,0:T(4,128)}, u32[]{:S(2)}) copy-start(f32[8,4,512]{2,1,0:T(4,128)} %param.21) | copy-start | bytes 196612
  8.0 4.6 %copy-start.4 = (bf16[8,4,512]{2,1,0:T(4,128)(2,1)S(1)}, bf16[8,4,512]{2,1,0:T(4,128)(2,1)}, u32[]{:S(2)}) copy-start(bf16[8,4,512]{2,1,0:T(4,128)(2,1)} %param.22) | copy-start | bytes 98308
  8.0 4.6 %copy-start.2 = (bf16[256,512]{1,0:T(8,128)(2,1)S(1)}, bf16[256,512]{1,0:T(8,128)(2,1)}, u32[]{:S(2)}) copy-start(bf16[256,512]{1,0:T(8,128)(2,1)} %param.12) | copy-start | bytes 786436
  11.2 24.9 %copy-start.7 = (s32[8]{0:T(128)S(1)}, s32[8]{0:T(128)}, u32[]{:S(2)}) copy-start(s32[8]{0:T(128)} %param.23) | copy-start | bytes 100
  11.2 25.0 %copy-start.5 = (f32[512]{0:T(512)S(1)}, f32[512]{0:T(512)}, u32[]{:S(2)}) copy-start(f32[512]{0:T(512)} %param.17) | copy-start | bytes 6148
  11.2 141.2 %reduce-scatter.7.cloned.1.call-start = ((), (), s32[]{:S(2)}) async-start(), calls=%async_computation.3 | async-start | bytes 327680
  43.2 51.0 %copy-start.1 = (f32[8,4,128,128]{3,2,1,0:T(8,128)}, f32[8,4,128,128]{3,2,1,0:T(8,128)S(1)}, u32[]{:S(2)}) copy-start(f32[8,4,128,128]{3,2,1,0:T(8,128)S(1)} %add_select_fusion) | copy-start | bytes 6291460
  94.3 7.5 %copy-start.6 = (f32[512]{0:T(512)S(1)}, f32[512]{0:T(512)}, u32[]{:S(2)}) copy-start(f32[512]{0:T(512)} %param.18) | copy-start | bytes 6148
Sparse Core Ops, SparseCore 0:
  11.4 68.4 reduce-scatter.4
  133.8 18.5 reduce-scatter.6
where the time goes:
time: 161 us
  waiting for transfers between devices  55.4 us (34%)
  blocking collectives  54 us (34%)
  matrix products  23.8 us (15%)
  between operations  14.9 us (9%)
  other arithmetic  9.3 us (6%)
  local copies, waits for them, and re-layouts  3.25 us (2%)
    reduce_scatter x1, waiting for transfers between devices, body(): lax.psum_scatter(terms, 'kv', scatter_dimension=0, tiled=True)  36.6 us
    all_gather x1, blocking collectives, body(): lax.all_gather(normed, 'kv', axis=0, tiled=True)  30.7 us
    unnamed x1, blocking collectives  23.3 us
    dot_general x4, matrix products, recurrence(): jnp.einsum('shk,shkv->shv', queries[:, position], carried, precision=lax....  20.3 us
    unnamed x3, waiting for transfers between devices  18.8 us
    select_n x1, other arithmetic, recurrence(): carried = jnp.where(taken_up, folded, carried)  7.01 us
  transfers between devices with their start and end apart: 2, of which 2 were waited for; matrix products, arithmetic and copies ran while one was open for 5% of the time, Pallas kernels for 0%

commit v1 on v0

v1 whole, which is shorter than its diff:
```python
import functools

import jax
import jax.numpy as jnp
from jax import lax
from jax.experimental import pallas as pl
from jax.experimental.pallas import tpu as pltpu
from jax.sharding import PartitionSpec as P

EPSILON = 1e-06
MESH = pl.DeviceIdType.MESH
INNER = 2


def kernel(
    nkv,
    ntp,
    x_hbm,
    gain_hbm,
    wq_hbm,
    wf_hbm,
    wv_hbm,
    low_hbm,
    hgain_hbm,
    wout_hbm,
    state_hbm,
    gate_hbm,
    oldv_hbm,
    out_ref,
    base_hbm,
    x,
    gain,
    w,
    low,
    hgain,
    wout,
    state,
    stateb,
    gate,
    oldv,
    xs,
    sq_out,
    sq_in,
    a_out,
    a_in,
    keep,
    b_out,
    b_in,
    ag,
    t_out,
    t_in,
    load_sem,
    base_sem,
    sq_send,
    sq_recv,
    a_send,
    a_recv,
    b_send,
    b_recv,
    gz_send,
    gz_recv,
    gy_send,
    gy_recv,
    t_send,
    t_recv,
):
    nz = nkv // INNER
    heads, depth, width3 = w.shape
    size = width3 // 3
    rows = x.shape[2]
    seqs = state.shape[0]
    props = rows // seqs
    features = depth * nkv
    f32 = jnp.float32
    bf16 = jnp.bfloat16

    kv = lax.axis_index("kv")
    tp = lax.axis_index("tp")
    z = kv // INNER
    y = kv % INNER
    other = 1 - y

    def kv_at(d):
        return lax.rem(kv + d, nkv)

    def tp_at(d):
        return lax.rem(tp + d, ntp)

    def z_at(d):
        return lax.rem(z + d, nz)

    barrier = pltpu.get_barrier_semaphore()
    for d in range(1, nkv):
        pl.semaphore_signal(barrier, inc=1, device_id={"kv": kv_at(d)}, device_id_type=MESH)
    for d in range(1, ntp):
        pl.semaphore_signal(barrier, inc=1, device_id={"tp": tp_at(d)}, device_id_type=MESH)

    loads = {}

    def load(name, src, dst):
        copy = pltpu.make_async_copy(src, dst, load_sem.at[len(loads)])
        copy.start()
        loads[name] = copy

    load("x", x_hbm, x)
    load("gain", gain_hbm, gain)
    for h in range(heads):
        for n, src in enumerate((wq_hbm, wf_hbm, wv_hbm)):
            load(
                ("w", h, n),
                src.at[:, pl.ds(h * size, size)],
                w.at[h, :, pl.ds(n * size, size)],
            )
    load("gate", gate_hbm, gate)
    load("oldv", oldv_hbm, oldv)
    for h in range(heads):
        load(("state", h), state_hbm.at[:, h], state.at[:, h])
    load("low", low_hbm, low)
    load("hgain", hgain_hbm, hgain)
    load("wout", wout_hbm, wout)

    loads["x"].wait()
    loads["gain"].wait()
    eye = lax.broadcasted_iota(jnp.int32, (rows, size), 0) == lax.broadcasted_iota(
        jnp.int32, (rows, size), 1
    )
    gain_row = gain[...].astype(f32)
    for zz in range(nz):
        for yy in range(INNER):
            block = x[zz, yy].astype(f32)
            xs[zz, yy] = (block * gain_row).astype(bf16)
            column = jnp.sum(block * block, axis=1, keepdims=True)
            row = jnp.sum(jnp.where(eye, column, 0.0), axis=0, keepdims=True)
            sq_out[zz * INNER + yy] = jnp.broadcast_to(row, (8, size))

    xs_other = xs[:, other].reshape(nz * rows, depth)
    xs_mine = xs[:, y].reshape(nz * rows, depth)
    a_copies = []
    sq_copies = []
    for h in range(heads):
        for n in range(3):
            loads[("w", h, n)].wait()
        part = jnp.dot(xs_other, w[h], preferred_element_type=f32)
        a_out[h] = part.astype(bf16).reshape(nz, rows, width3)
        if h == 0:
            pl.semaphore_wait(barrier, nkv - 1 + ntp - 1)
            for d in range(1, nkv):
                copy = pltpu.make_async_remote_copy(
                    src_ref=sq_out.at[kv_at(d)],
                    dst_ref=sq_in.at[d - 1],
                    send_sem=sq_send.at[d - 1],
                    recv_sem=sq_recv.at[d - 1],
                    device_id={"kv": kv_at(d)},
                    device_id_type=MESH,
                )
                copy.start()
                sq_copies.append(copy)
        copy = pltpu.make_async_remote_copy(
            src_ref=a_out.at[h],
            dst_ref=a_in.at[h],
            send_sem=a_send.at[h],
            recv_sem=a_recv.at[h],
            device_id={"kv": z * INNER + other},
            device_id_type=MESH,
        )
        copy.start()
        a_copies.append(copy)
    for h in range(heads):
        part = jnp.dot(xs_mine, w[h], preferred_element_type=f32)
        keep[h] = part.reshape(nz, rows, width3)

    loads["gate"].wait()
    loads["oldv"].wait()
    gates = jnp.concatenate(
        [gate[:, h * size : (h + 1) * size] for h in range(heads)], axis=0
    )
    gates_t = gates.T
    base_copies = []
    b_copies = []
    for h in range(heads):
        loads[("state", h)].wait()
        for s in range(seqs):
            carried = state[s, h]
            for j in range(props):
                at = h * rows + s * props + j
                g = gates_t[:, at : at + 1]
                v = oldv[s * props + j : s * props + j + 1, h * size : (h + 1) * size]
                carried = g * carried + (1.0 - g) * v
            state[s, h] = carried
            stateb[s, h] = carried.astype(bf16)
        copy = pltpu.make_async_copy(state.at[:, h], base_hbm.at[:, h], base_sem.at[h])
        copy.start()
        base_copies.append(copy)

        a_copies[h].wait_recv()
        row_copies = []
        for d in range(1, nz):
            to = z_at(d)
            b_out[h, d - 1] = (keep[h, to] + a_in[h, to].astype(f32)).astype(bf16)
            copy = pltpu.make_async_remote_copy(
                src_ref=b_out.at[h, d - 1],
                dst_ref=b_in.at[h, d - 1],
                send_sem=b_send.at[h, d - 1],
                recv_sem=b_recv.at[h, d - 1],
                device_id={"kv": to * INNER + y},
                device_id_type=MESH,
            )
            copy.start()
            row_copies.append(copy)
        b_copies.append(row_copies)

    total = sq_out[kv]
    for d in range(1, nkv):
        sq_copies[d - 1].wait_recv()
        total = total + sq_in[d - 1]
    column = jnp.sum(jnp.where(eye, total[0:1], 0.0), axis=1, keepdims=True)
    rscale = lax.rsqrt(column / features + EPSILON)

    loads["low"].wait()
    loads["hgain"].wait()
    place = lax.broadcasted_iota(jnp.int32, (rows, size), 0)
    position = place % props
    half = lax.broadcasted_iota(jnp.int32, (8, size), 0) // props
    for h in range(heads):
        mine = keep[h, z] + a_in[h, z].astype(f32)
        for d in range(1, nz):
            b_copies[h][d - 1].wait_recv()
            mine = mine + b_in[h, d - 1].astype(f32)
        mine = mine * rscale
        query = mine[:, :size]
        query = query / (1.0 + jnp.exp(-query))
        floor = low[:, h * size : (h + 1) * size]
        forget = floor + (1.0 - floor) * jax.nn.sigmoid(mine[:, size : 2 * size])
        key = 1.0 - forget
        value = mine[:, 2 * size :]
        decay = query
        head_out = jnp.sum(query * key, axis=1, keepdims=True) * value
        for d in range(1, props):
            earlier = forget if d == 1 else pltpu.roll(forget, d - 1, 0)
            decay = decay * jnp.where(position >= d - 1, earlier, 1.0)
            weight = jnp.where(position >= d, decay * pltpu.roll(key, d, 0), 0.0)
            head_out = head_out + jnp.sum(weight, axis=1, keepdims=True) * pltpu.roll(
                value, d, 0
            )
        decay = decay * jnp.where(position >= props - 1, pltpu.roll(forget, props - 1, 0), 1.0)
        decay = decay.astype(bf16)
        per = 8 // props
        pieces = []
        for r in range(rows // 8):
            left = decay[r * 8 : (r + 1) * 8]
            piece = jnp.zeros((8, size), f32)
            for k in range(per):
                product = jnp.dot(left, stateb[r * per + k, h], preferred_element_type=f32)
                piece = jnp.where(half == k, product, piece)
            pieces.append(piece)
        head_out = head_out + jnp.concatenate(pieces, axis=0)
        mean = jnp.mean(head_out * head_out, axis=1, keepdims=True)
        normed = head_out * lax.rsqrt(mean + EPSILON) * hgain[:, h * size : (h + 1) * size]
        ag[z, y, :, h * size : (h + 1) * size] = normed.astype(bf16)

    def to_inner(slot, zz):
        copy = pltpu.make_async_remote_copy(
            src_ref=ag.at[zz, y],
            dst_ref=ag.at[zz, y],
            send_sem=gy_send.at[slot],
            recv_sem=gy_recv.at[slot],
            device_id={"kv": z * INNER + other},
            device_id_type=MESH,
        )
        copy.start()
        return copy

    gz_copies = []
    for d in range(1, nz):
        copy = pltpu.make_async_remote_copy(
            src_ref=ag.at[z, y],
            dst_ref=ag.at[z, y],
            send_sem=gz_send.at[d - 1],
            recv_sem=gz_recv.at[d - 1],
            device_id={"kv": z_at(d) * INNER + y},
            device_id_type=MESH,
        )
        copy.start()
        gz_copies.append(copy)
    gy_copies = [to_inner(0, z)]
    for d in range(1, nz):
        gz_copies[d - 1].wait_recv()
        gy_copies.append(to_inner(d, z_at(nz - d)))

    loads["wout"].wait()
    t_copies = []
    cols = out_ref.shape[3]
    for g in range(2):
        side = y if g == 0 else other
        if g == 1:
            for copy in gy_copies:
                copy.wait_recv()
        left = ag[:, side].reshape(nz * rows, heads * size)
        part = jnp.dot(left, wout[...], preferred_element_type=f32).astype(bf16)
        for t in range(ntp):
            t_out[g, t] = part[:, t * cols : (t + 1) * cols].reshape(nz, rows, cols)
        for d in range(1, ntp):
            copy = pltpu.make_async_remote_copy(
                src_ref=t_out.at[g, tp_at(d)],
                dst_ref=t_in.at[g, d - 1],
                send_sem=t_send.at[g, d - 1],
                recv_sem=t_recv.at[g, d - 1],
                device_id={"tp": tp_at(d)},
                device_id_type=MESH,
            )
            copy.start()
            t_copies.append(copy)
    for g in range(2):
        side = y if g == 0 else other
        acc = t_out[g, tp].astype(f32)
        for d in range(1, ntp):
            t_copies[g * (ntp - 1) + d - 1].wait_recv()
            acc = acc + t_in[g, d - 1].astype(f32)
        out_ref[:, side] = acc.astype(bf16)

    for copy in base_copies:
        copy.wait()
    for copy in sq_copies + a_copies + sum(b_copies, []) + gz_copies + gy_copies + t_copies:
        copy.wait_send()


def body(
    nkv,
    ntp,
    inputs,
    norm_gain,
    w_query,
    w_forget,
    w_value,
    lower_bound,
    head_gain,
    w_out,
    prior_state,
    prev_forget,
    prev_values,
    accepted,
):
    tokens, depth = inputs.shape
    seqs, heads, size, _ = prior_state.shape
    props = prev_forget.shape[1]
    rows = seqs * props
    width = heads * size
    nz = nkv // INNER
    cols = w_out.shape[1] // ntp
    taken = jnp.arange(props)[None, :, None] < accepted[:, None, None]
    gate = jnp.where(taken, prev_forget, 1.0).reshape(rows, width)
    oldv = prev_values.astype(jnp.float32).reshape(rows, width)
    f32, bf16 = jnp.float32, jnp.bfloat16
    dma = pltpu.SemaphoreType.DMA
    anywhere = pl.BlockSpec(memory_space=pl.ANY)
    mixed, base = pl.pallas_call(
        functools.partial(kernel, nkv, ntp),
        out_shape=(
            jax.ShapeDtypeStruct((nz, INNER, rows, cols), bf16),
            jax.ShapeDtypeStruct(prior_state.shape, f32),
        ),
        in_specs=[anywhere] * 11,
        out_specs=(pl.BlockSpec(memory_space=pltpu.VMEM), anywhere),
        scratch_shapes=[
            pltpu.VMEM((nz, INNER, rows, depth), bf16),
            pltpu.VMEM((1, depth), bf16),
            pltpu.VMEM((heads, depth, 3 * size), bf16),
            pltpu.VMEM((1, width), f32),
            pltpu.VMEM((1, width), f32),
            pltpu.VMEM(w_out.shape, bf16),
            pltpu.VMEM(prior_state.shape, f32),
            pltpu.VMEM(prior_state.shape, bf16),
            pltpu.VMEM((rows, width), f32),
            pltpu.VMEM((rows, width), f32),
            pltpu.VMEM((nz, INNER, rows, depth), bf16),
            pltpu.VMEM((nkv, 8, size), f32),
            pltpu.VMEM((nkv - 1, 8, size), f32),
            pltpu.VMEM((heads, nz, rows, 3 * size), bf16),
            pltpu.VMEM((heads, nz, rows, 3 * size), bf16),
            pltpu.VMEM((heads, nz, rows, 3 * size), f32),
            pltpu.VMEM((heads, nz - 1, rows, 3 * size), bf16),
            pltpu.VMEM((heads, nz - 1, rows, 3 * size), bf16),
            pltpu.VMEM((nz, INNER, rows, width), bf16),
            pltpu.VMEM((2, ntp, nz, rows, cols), bf16),
            pltpu.VMEM((2, ntp - 1, nz, rows, cols), bf16),
            dma((8 + 4 * heads,)),
            dma((heads,)),
            dma((nkv - 1,)),
            dma((nkv - 1,)),
            dma((heads,)),
            dma((heads,)),
            dma((heads, nz - 1)),
            dma((heads, nz - 1)),
            dma((nz - 1,)),
            dma((nz - 1,)),
            dma((nz,)),
            dma((nz,)),
            dma((2, ntp - 1)),
            dma((2, ntp - 1)),
        ],
        compiler_params=pltpu.CompilerParams(
            collective_id=0, has_side_effects=True, vmem_limit_bytes=60 * 1024 * 1024
        ),
    )(
        inputs.reshape(nz, INNER, rows, depth),
        norm_gain.reshape(1, depth),
        w_query,
        w_forget,
        w_value,
        lower_bound.reshape(1, width),
        head_gain.reshape(1, width),
        w_out,
        prior_state,
        gate,
        oldv,
    )
    return mixed.reshape(tokens, cols), base


def solution(mesh):
    in_specs = (
        P(None, "kv"),
        P("kv"),
        P("kv", "tp"),
        P("kv", "tp"),
        P("kv", "tp"),
        P("tp"),
        P("tp"),
        P("tp", "kv"),
        P("kv", "tp", None, None),
        P("kv", None, "tp"),
        P("kv", None, "tp"),
        P("kv"),
    )
    out_specs = (P(None, ("kv", "tp")), P("kv", "tp", None, None))
    return jax.shard_map(
        functools.partial(body, mesh.shape["kv"], mesh.shape["tp"]),
        mesh=mesh,
        in_specs=in_specs,
        out_specs=out_specs,
        check_vma=False,
    )
```

time: 161 us -> 44.2 us (0.27)
  waiting for transfers between devices: 55.4 us -> 0 us
  blocking collectives: 54 us -> 0 us
  Pallas kernels: 0 us -> 33.7 us
  matrix products: 23.8 us -> 0 us
  between operations: 14.9 us -> 0.64 us
  other arithmetic: 9.3 us -> 1.65 us
  local copies, waits for them, and re-layouts: 3.25 us -> 7.91 us
    reduce_scatter x1 -> x0, waiting for transfers between devices: 36.6 us -> none  [body(): lax.psum_scatter(terms, 'kv', scatter_dimension=0, tiled=True)]
    pallas_call x0 -> x1, Pallas kernels: none -> 33.7 us  [body(): pl.pallas_call(functools.partial(kernel, nkv, ntp), out_shape=(jax.ShapeD...]
    all_gather x1 -> x0, blocking collectives: 30.7 us -> none  [body(): lax.all_gather(normed, 'kv', axis=0, tiled=True)]
    dot_general x6 -> x0, matrix products: 23.8 us -> none  [the longest x4 20.3 us: recurrence(): jnp.einsum('shk,shkv->shv', queries[:, position], carried, precision=lax....]
    unnamed x1 -> x0, blocking collectives: 23.3 us -> none
    unnamed x3 -> x0, waiting for transfers between devices: 18.8 us -> none
    select_n x1, other arithmetic: 7.01 us -> 0.92 us  [body(): gate = jnp.where(taken, prev_forget, 1.0).reshape(rows, width)]
    reshape x4 -> x3, local copies, waits for them, and re-layouts: 0.11 us -> 3.3 us  [the longest x1 1.39 us: body(): oldv = prev_values.astype(jnp.float32).reshape(rows, width)]
  transfers between devices with their start and end apart: 2 -> 0, of which waited for: 2 -> 0; matrix products, arithmetic and copies ran while one was open for 5% -> 0% of each run, Pallas kernels for 0% -> 0%
where the time goes in v1:
time: 44.2 us; the launch traced here: 43.9 us
  Pallas kernels  33.7 us (76%)
  local copies, waits for them, and re-layouts  7.91 us (18%)
  other arithmetic  1.65 us (4%)
  between operations  0.64 us (1%)
    pallas_call x1, Pallas kernels, body(): pl.pallas_call(functools.partial(kernel, nkv, ntp), out_shape=(jax.ShapeD...  33.7 us
    unnamed x2, local copies, waits for them, and re-layouts  4.61 us
    reshape x1, local copies, waits for them, and re-layouts, body(): oldv = prev_values.astype(jnp.float32).reshape(rows, width)  1.39 us
    reshape x1, local copies, waits for them, and re-layouts, body(): norm_gain.reshape(1, depth)  1.25 us
    select_n x1, other arithmetic, body(): gate = jnp.where(taken, prev_forget, 1.0).reshape(rows, width)  0.92 us

profile of v1, /device:TPU:0, one launch (start us, length us, event | category | flops | bytes accessed | tf_op | source)
XLA Modules:
  0.0 43.9 jit_solution(6028975012588106698)
XLA Ops:
  0.6 0.7 %iota_compare_fusion = pred[8,4]{1,0:T(8,128)(4,1)S(1)} fusion(s32[8]{0:T(128)} %param.23), kind=kLoop, calls=%fused_computation.1 | loop fusion | flops 32 | bytes 64 | tf_op jit(solution)/shard_map/lt | solution.py:350
  1.4 1.3 %reshape.53.gain_hbm = bf16[1,512]{1,0:T(2,128)(2,1)} reshape(bf16[512]{0:T(512)(128)(2,1)} %param.13) | data formatting | bytes 2048 | tf_op jit(solution)/shard_map/reshape | solution.py:406
  2.6 0.9 %broadcast_select_fusion = f32[8,4,512]{2,1,0:T(4,128)S(1)} fusion(f32[8,4,512]{2,1,0:T(4,128)} %param.21, pred[8,4]{1,0:T(8,128)(4,1)S(1)} %iota_compare_fusion), kind=kLoop, calls=%fused_computation | loop fusion | flops 16384 | bytes 131104 | tf_op jit(solution)/shard_map/jit(_where)/select_n | solution.py:351
  3.5 0.7 %reshape.56.gate_hbm = f32[32,512]{1,0:T(8,128)} reshape(f32[8,4,512]{2,1,0:T(4,128)S(1)} %broadcast_select_fusion) | data formatting | bytes 131072 | tf_op jit(solution)/shard_map/reshape | solution.py:351
  4.2 1.4 %reshape.61.oldv_hbm = f32[32,512]{1,0:T(8,128)} reshape(bf16[8,4,512]{2,1,0:T(4,128)(2,1)} %param.22) | data formatting | bytes 98304 | tf_op jit(solution)/shard_map/reshape | solution.py:352
  5.6 33.7 %shard_map.131 = (bf16[4,2,32,128]{3,2,1,0:T(8,128)(2,1)}, f32[8,4,128,128]{3,2,1,0:T(8,128)}) custom-call(bf16[4,2,32,512]{3,2,1,0:T(8,128)(2,1)} %bitcast.4, bf16[1,512]{1,0:T(2,128)(2,1)} %reshape.53.gain_hbm, bf16[512,512]{1,0:T(8,128)(2,1)} %wq_hbm.1, bf16[512,512]{1,0:T(8,128)(2,1)} %wf_hbm.1, bf16[512,512]{1,0:T(8,128)(2,1)} %wv_hbm.1, ...), custom_call_target="tpu_custom_call" | custom-call | tf_op jit(solution)/shard_map/pallas_call | solution.py:356
  39.2 1.5 %copy.16 = bf16[256,128]{1,0:T(8,128)(2,1)} copy(bf16[256,128]{1,0:T(8,128)(2,1)} %bitcast.5) | data formatting | bytes 131072
  40.7 3.1 %copy.17 = f32[8,4,128,128]{3,2,1,0:T(8,128)} copy(f32[8,4,128,128]{3,2,1,0:T(8,128)} %get-tuple-element.9) | data formatting | bytes 4194304

commit v2 on v1

--- a/solution.py
+++ b/solution.py
@@ -26,6 +26,7 @@
     state_hbm,
     gate_hbm,
     oldv_hbm,
+    accepted,
     out_ref,
     base_hbm,
     x,
@@ -37,6 +38,7 @@
     state,
     stateb,
     gate,
+    gates,
     oldv,
     xs,
     sq_out,
@@ -57,10 +59,8 @@
     a_recv,
     b_send,
     b_recv,
-    gz_send,
-    gz_recv,
-    gy_send,
-    gy_recv,
+    g_send,
+    g_recv,
     t_send,
     t_recv,
 ):
@@ -124,7 +124,7 @@
     eye = lax.broadcasted_iota(jnp.int32, (rows, size), 0) == lax.broadcasted_iota(
         jnp.int32, (rows, size), 1
     )
-    gain_row = gain[...].astype(f32)
+    gain_row = gain[...].astype(f32).reshape(1, depth)
     for zz in range(nz):
         for yy in range(INNER):
             block = x[zz, yy].astype(f32)
@@ -171,21 +171,23 @@
 
     loads["gate"].wait()
     loads["oldv"].wait()
-    gates = jnp.concatenate(
-        [gate[:, h * size : (h + 1) * size] for h in range(heads)], axis=0
-    )
-    gates_t = gates.T
+    order = lax.broadcasted_iota(jnp.int32, (props, heads * size), 0)
+    for s in range(seqs):
+        kept = jnp.where(order < accepted[s], gate[s], 1.0)
+        for h in range(heads):
+            gates[pl.ds(h * rows + s * props, props), :] = kept[:, h * size : (h + 1) * size]
+    gates_t = gates[...].T
     base_copies = []
     b_copies = []
     for h in range(heads):
         loads[("state", h)].wait()
         for s in range(seqs):
             carried = state[s, h]
+            values = oldv[s, :, h * size : (h + 1) * size].astype(f32)
             for j in range(props):
                 at = h * rows + s * props + j
                 g = gates_t[:, at : at + 1]
-                v = oldv[s * props + j : s * props + j + 1, h * size : (h + 1) * size]
-                carried = g * carried + (1.0 - g) * v
+                carried = g * carried + (1.0 - g) * values[j : j + 1]
             state[s, h] = carried
             stateb[s, h] = carried.astype(bf16)
         copy = pltpu.make_async_copy(state.at[:, h], base_hbm.at[:, h], base_sem.at[h])
@@ -221,6 +223,25 @@
     place = lax.broadcasted_iota(jnp.int32, (rows, size), 0)
     position = place % props
     half = lax.broadcasted_iota(jnp.int32, (8, size), 0) // props
+    g_copies = []
+
+    def share(h, slot, zz, to):
+        copy = pltpu.make_async_remote_copy(
+            src_ref=ag.at[h, zz, y],
+            dst_ref=ag.at[h, zz, y],
+            send_sem=g_send.at[h, slot],
+            recv_sem=g_recv.at[h, slot],
+            device_id={"kv": to},
+            device_id_type=MESH,
+        )
+        copy.start()
+        return copy
+
+    def pass_on(h):
+        for d in range(1, nz):
+            g_copies[h][d].wait_recv()
+            g_copies[h].append(share(h, nz + d - 1, z_at(nz - d), z * INNER + other))
+
     for h in range(heads):
         mine = keep[h, z] + a_in[h, z].astype(f32)
         for d in range(1, nz):
@@ -256,47 +277,31 @@
         head_out = head_out + jnp.concatenate(pieces, axis=0)
         mean = jnp.mean(head_out * head_out, axis=1, keepdims=True)
         normed = head_out * lax.rsqrt(mean + EPSILON) * hgain[:, h * size : (h + 1) * size]
-        ag[z, y, :, h * size : (h + 1) * size] = normed.astype(bf16)
-
-    def to_inner(slot, zz):
-        copy = pltpu.make_async_remote_copy(
-            src_ref=ag.at[zz, y],
-            dst_ref=ag.at[zz, y],
-            send_sem=gy_send.at[slot],
-            recv_sem=gy_recv.at[slot],
-            device_id={"kv": z * INNER + other},
-            device_id_type=MESH,
-        )
-        copy.start()
-        return copy
-
-    gz_copies = []
-    for d in range(1, nz):
-        copy = pltpu.make_async_remote_copy(
-            src_ref=ag.at[z, y],
-            dst_ref=ag.at[z, y],
-            send_sem=gz_send.at[d - 1],
-            recv_sem=gz_recv.at[d - 1],
-            device_id={"kv": z_at(d) * INNER + y},
-            device_id_type=MESH,
-        )
-        copy.start()
-        gz_copies.append(copy)
-    gy_copies = [to_inner(0, z)]
-    for d in range(1, nz):
-        gz_copies[d - 1].wait_recv()
-        gy_copies.append(to_inner(d, z_at(nz - d)))
+        ag[h, z, y] = normed.astype(bf16)
+        copies = [share(h, 0, z, z * INNER + other)]
+        for d in range(1, nz):
+            copies.append(share(h, d, z, z_at(d) * INNER + y))
+        g_copies.append(copies)
+        if h:
+            pass_on(h - 1)
+    pass_on(heads - 1)
 
     loads["wout"].wait()
     t_copies = []
     cols = out_ref.shape[3]
     for g in range(2):
         side = y if g == 0 else other
-        if g == 1:
-            for copy in gy_copies:
-                copy.wait_recv()
-        left = ag[:, side].reshape(nz * rows, heads * size)
-        part = jnp.dot(left, wout[...], preferred_element_type=f32).astype(bf16)
+        part = jnp.zeros((nz * rows, ntp * cols), f32)
+        for h in range(heads):
+            if g == 1:
+                g_copies[h][0].wait_recv()
+                for copy in g_copies[h][nz:]:
+                    copy.wait_recv()
+            left = ag[h, :, side].reshape(nz * rows, size)
+            part = part + jnp.dot(
+                left, wout[h * size : (h + 1) * size], preferred_element_type=f32
+            )
+        part = part.astype(bf16)
         for t in range(ntp):
             t_out[g, t] = part[:, t * cols : (t + 1) * cols].reshape(nz, rows, cols)
         for d in range(1, ntp):
@@ -320,7 +325,7 @@
 
     for copy in base_copies:
         copy.wait()
-    for copy in sq_copies + a_copies + sum(b_copies, []) + gz_copies + gy_copies + t_copies:
+    for copy in sq_copies + a_copies + sum(b_copies, []) + sum(g_copies, []) + t_copies:
         copy.wait_send()
 
 
@@ -347,9 +352,6 @@
     width = heads * size
     nz = nkv // INNER
     cols = w_out.shape[1] // ntp
-    taken = jnp.arange(props)[None, :, None] < accepted[:, None, None]
-    gate = jnp.where(taken, prev_forget, 1.0).reshape(rows, width)
-    oldv = prev_values.astype(jnp.float32).reshape(rows, width)
     f32, bf16 = jnp.float32, jnp.bfloat16
     dma = pltpu.SemaphoreType.DMA
     anywhere = pl.BlockSpec(memory_space=pl.ANY)
@@ -359,19 +361,20 @@
             jax.ShapeDtypeStruct((nz, INNER, rows, cols), bf16),
             jax.ShapeDtypeStruct(prior_state.shape, f32),
         ),
-        in_specs=[anywhere] * 11,
+        in_specs=[anywhere] * 11 + [pl.BlockSpec(memory_space=pltpu.SMEM)],
         out_specs=(pl.BlockSpec(memory_space=pltpu.VMEM), anywhere),
         scratch_shapes=[
             pltpu.VMEM((nz, INNER, rows, depth), bf16),
-            pltpu.VMEM((1, depth), bf16),
+            pltpu.VMEM((depth,), bf16),
             pltpu.VMEM((heads, depth, 3 * size), bf16),
             pltpu.VMEM((1, width), f32),
             pltpu.VMEM((1, width), f32),
             pltpu.VMEM(w_out.shape, bf16),
             pltpu.VMEM(prior_state.shape, f32),
             pltpu.VMEM(prior_state.shape, bf16),
-            pltpu.VMEM((rows, width), f32),
-            pltpu.VMEM((rows, width), f32),
+            pltpu.VMEM(prev_forget.shape, f32),
+            pltpu.VMEM((heads * rows, size), f32),
+            pltpu.VMEM(prev_values.shape, bf16),
             pltpu.VMEM((nz, INNER, rows, depth), bf16),
             pltpu.VMEM((nkv, 8, size), f32),
             pltpu.VMEM((nkv - 1, 8, size), f32),
@@ -380,7 +383,7 @@
             pltpu.VMEM((heads, nz, rows, 3 * size), f32),
             pltpu.VMEM((heads, nz - 1, rows, 3 * size), bf16),
             pltpu.VMEM((heads, nz - 1, rows, 3 * size), bf16),
-            pltpu.VMEM((nz, INNER, rows, width), bf16),
+            pltpu.VMEM((heads, nz, INNER, rows, size), bf16),
             pltpu.VMEM((2, ntp, nz, rows, cols), bf16),
             pltpu.VMEM((2, ntp - 1, nz, rows, cols), bf16),
             dma((8 + 4 * heads,)),
@@ -391,10 +394,8 @@
             dma((heads,)),
             dma((heads, nz - 1)),
             dma((heads, nz - 1)),
-            dma((nz - 1,)),
-            dma((nz - 1,)),
-            dma((nz,)),
-            dma((nz,)),
+            dma((heads, 2 * nz - 1)),
+            dma((heads, 2 * nz - 1)),
             dma((2, ntp - 1)),
             dma((2, ntp - 1)),
         ],
@@ -403,7 +404,7 @@
         ),
     )(
         inputs.reshape(nz, INNER, rows, depth),
-        norm_gain.reshape(1, depth),
+        norm_gain,
         w_query,
         w_forget,
         w_value,
@@ -411,8 +412,9 @@
         head_gain.reshape(1, width),
         w_out,
         prior_state,
-        gate,
-        oldv,
+        prev_forget,
+        prev_values,
+        accepted,
     )
     return mixed.reshape(tokens, cols), base
 

time: 44.2 us -> 40.9 us (0.925)
  local copies, waits for them, and re-layouts: 7.91 us -> 4.61 us
  Pallas kernels: 33.7 us -> 35.4 us
  other arithmetic: 1.65 us -> 0 us
    reshape x3 -> x0, local copies, waits for them, and re-layouts: 3.3 us -> none  [the longest x1 1.39 us: body(): oldv = prev_values.astype(jnp.float32).reshape(rows, width)]
    pallas_call x1, Pallas kernels: 33.7 us -> 35.4 us  [body(): pl.pallas_call(functools.partial(kernel, nkv, ntp), out_shape=(jax.ShapeD...]
    select_n x1 -> x0, other arithmetic: 0.92 us -> none  [body(): gate = jnp.where(taken, prev_forget, 1.0).reshape(rows, width)]
    lt x1 -> x0, other arithmetic: 0.73 us -> none  [body(): taken = jnp.arange(props)[None, :, None] < accepted[:, None, None]]
where the time goes in v2:
time: 40.9 us; the launch traced here: 40.6 us
  Pallas kernels  35.4 us (87%)
  local copies, waits for them, and re-layouts  4.61 us (11%)
  between operations  0.64 us (2%)
    pallas_call x1, Pallas kernels, body(): pl.pallas_call(functools.partial(kernel, nkv, ntp), out_shape=(jax.ShapeD...  35.4 us
    unnamed x2, local copies, waits for them, and re-layouts  4.61 us

profile of v2, /device:TPU:0, one launch (start us, length us, event | category | flops | bytes accessed | tf_op | source)
XLA Modules:
  0.0 40.6 jit_solution(1864709947871478907)
XLA Ops:
  0.6 35.4 %shard_map.131 = (bf16[4,2,32,128]{3,2,1,0:T(8,128)(2,1)}, f32[8,4,128,128]{3,2,1,0:T(8,128)}) custom-call(bf16[4,2,32,512]{3,2,1,0:T(8,128)(2,1)} %bitcast.4, bf16[512]{0:T(512)(128)(2,1)} %gain_hbm.1, bf16[512,512]{1,0:T(8,128)(2,1)} %wq_hbm.1, bf16[512,512]{1,0:T(8,128)(2,1)} %wf_hbm.1, bf16[512,512]{1,0:T(8,128)(2,1)} %wv_hbm.1, f32[1,512]{1,0:T(1,128)} %bitcast.6, ...), custom_call_target="tpu_custom_call" | custom-call | tf_op jit(solution)/shard_map/pallas_call | solution.py:358
  36.0 1.5 %copy.16 = bf16[256,128]{1,0:T(8,128)(2,1)} copy(bf16[256,128]{1,0:T(8,128)(2,1)} %bitcast.5) | data formatting | bytes 131072
  37.5 3.1 %copy.17 = f32[8,4,128,128]{3,2,1,0:T(8,128)} copy(f32[8,4,128,128]{3,2,1,0:T(8,128)} %get-tuple-element.9) | data formatting | bytes 4194304

commit v3 on v2

--- a/solution.py
+++ b/solution.py
@@ -1,4 +1,5 @@
 import functools
+import math
 
 import jax
 import jax.numpy as jnp
@@ -26,9 +27,9 @@
     state_hbm,
     gate_hbm,
     oldv_hbm,
-    accepted,
+    accepted_hbm,
     out_ref,
-    base_hbm,
+    base,
     x,
     gain,
     w,
@@ -40,6 +41,7 @@
     gate,
     gates,
     oldv,
+    accepted,
     xs,
     sq_out,
     sq_in,
@@ -52,7 +54,6 @@
     t_out,
     t_in,
     load_sem,
-    base_sem,
     sq_send,
     sq_recv,
     a_send,
@@ -113,6 +114,7 @@
             )
     load("gate", gate_hbm, gate)
     load("oldv", oldv_hbm, oldv)
+    load("accepted", accepted_hbm, accepted)
     for h in range(heads):
         load(("state", h), state_hbm.at[:, h], state.at[:, h])
     load("low", low_hbm, low)
@@ -171,13 +173,13 @@
 
     loads["gate"].wait()
     loads["oldv"].wait()
+    loads["accepted"].wait()
     order = lax.broadcasted_iota(jnp.int32, (props, heads * size), 0)
     for s in range(seqs):
         kept = jnp.where(order < accepted[s], gate[s], 1.0)
         for h in range(heads):
             gates[pl.ds(h * rows + s * props, props), :] = kept[:, h * size : (h + 1) * size]
     gates_t = gates[...].T
-    base_copies = []
     b_copies = []
     for h in range(heads):
         loads[("state", h)].wait()
@@ -188,11 +190,8 @@
                 at = h * rows + s * props + j
                 g = gates_t[:, at : at + 1]
                 carried = g * carried + (1.0 - g) * values[j : j + 1]
-            state[s, h] = carried
+            base[s, h] = carried
             stateb[s, h] = carried.astype(bf16)
-        copy = pltpu.make_async_copy(state.at[:, h], base_hbm.at[:, h], base_sem.at[h])
-        copy.start()
-        base_copies.append(copy)
 
         a_copies[h].wait_recv()
         row_copies = []
@@ -323,8 +322,6 @@
             acc = acc + t_in[g, d - 1].astype(f32)
         out_ref[:, side] = acc.astype(bf16)
 
-    for copy in base_copies:
-        copy.wait()
     for copy in sq_copies + a_copies + sum(b_copies, []) + sum(g_copies, []) + t_copies:
         copy.wait_send()
 
@@ -355,52 +352,55 @@
     f32, bf16 = jnp.float32, jnp.bfloat16
     dma = pltpu.SemaphoreType.DMA
     anywhere = pl.BlockSpec(memory_space=pl.ANY)
+    scratch = [
+        pltpu.VMEM((nz, INNER, rows, depth), bf16),
+        pltpu.VMEM((depth,), bf16),
+        pltpu.VMEM((heads, depth, 3 * size), bf16),
+        pltpu.VMEM((1, width), f32),
+        pltpu.VMEM((1, width), f32),
+        pltpu.VMEM(w_out.shape, bf16),
+        pltpu.VMEM(prior_state.shape, f32),
+        pltpu.VMEM(prior_state.shape, bf16),
+        pltpu.VMEM(prev_forget.shape, f32),
+        pltpu.VMEM((heads * rows, size), f32),
+        pltpu.VMEM(prev_values.shape, bf16),
+        pltpu.SMEM(accepted.shape, jnp.int32),
+        pltpu.VMEM((nz, INNER, rows, depth), bf16),
+        pltpu.VMEM((nkv, 8, size), f32),
+        pltpu.VMEM((nkv - 1, 8, size), f32),
+        pltpu.VMEM((heads, nz, rows, 3 * size), bf16),
+        pltpu.VMEM((heads, nz, rows, 3 * size), bf16),
+        pltpu.VMEM((heads, nz, rows, 3 * size), f32),
+        pltpu.VMEM((heads, nz - 1, rows, 3 * size), bf16),
+        pltpu.VMEM((heads, nz - 1, rows, 3 * size), bf16),
+        pltpu.VMEM((heads, nz, INNER, rows, size), bf16),
+        pltpu.VMEM((2, ntp, nz, rows, cols), bf16),
+        pltpu.VMEM((2, ntp - 1, nz, rows, cols), bf16),
+        dma((8 + 4 * heads,)),
+        dma((nkv - 1,)),
+        dma((nkv - 1,)),
+        dma((heads,)),
+        dma((heads,)),
+        dma((heads, nz - 1)),
+        dma((heads, nz - 1)),
+        dma((heads, 2 * nz - 1)),
+        dma((heads, 2 * nz - 1)),
+        dma((2, ntp - 1)),
+        dma((2, ntp - 1)),
+    ]
+    results = 4 * math.prod(prior_state.shape) + 2 * tokens * cols
+    limit = 61 * 1024 * 1024 - results
     mixed, base = pl.pallas_call(
         functools.partial(kernel, nkv, ntp),
         out_shape=(
-            jax.ShapeDtypeStruct((nz, INNER, rows, cols), bf16),
-            jax.ShapeDtypeStruct(prior_state.shape, f32),
+            pltpu.VMEM((nz, INNER, rows, cols), bf16),
+            pltpu.VMEM(prior_state.shape, f32),
         ),
-        in_specs=[anywhere] * 11 + [pl.BlockSpec(memory_space=pltpu.SMEM)],
-        out_specs=(pl.BlockSpec(memory_space=pltpu.VMEM), anywhere),
-        scratch_shapes=[
-            pltpu.VMEM((nz, INNER, rows, depth), bf16),
-            pltpu.VMEM((depth,), bf16),
-            pltpu.VMEM((heads, depth, 3 * size), bf16),
-            pltpu.VMEM((1, width), f32),
-            pltpu.VMEM((1, width), f32),
-            pltpu.VMEM(w_out.shape, bf16),
-            pltpu.VMEM(prior_state.shape, f32),
-            pltpu.VMEM(prior_state.shape, bf16),
-            pltpu.VMEM(prev_forget.shape, f32),
-            pltpu.VMEM((heads * rows, size), f32),
-            pltpu.VMEM(prev_values.shape, bf16),
-            pltpu.VMEM((nz, INNER, rows, depth), bf16),
-            pltpu.VMEM((nkv, 8, size), f32),
-            pltpu.VMEM((nkv - 1, 8, size), f32),
-            pltpu.VMEM((heads, nz, rows, 3 * size), bf16),
-            pltpu.VMEM((heads, nz, rows, 3 * size), bf16),
-            pltpu.VMEM((heads, nz, rows, 3 * size), f32),
-            pltpu.VMEM((heads, nz - 1, rows, 3 * size), bf16),
-            pltpu.VMEM((heads, nz - 1, rows, 3 * size), bf16),
-            pltpu.VMEM((heads, nz, INNER, rows, size), bf16),
-            pltpu.VMEM((2, ntp, nz, rows, cols), bf16),
-            pltpu.VMEM((2, ntp - 1, nz, rows, cols), bf16),
-            dma((8 + 4 * heads,)),
-            dma((heads,)),
-            dma((nkv - 1,)),
-            dma((nkv - 1,)),
-            dma((heads,)),
-            dma((heads,)),
-            dma((heads, nz - 1)),
-            dma((heads, nz - 1)),
-            dma((heads, 2 * nz - 1)),
-            dma((heads, 2 * nz - 1)),
-            dma((2, ntp - 1)),
-            dma((2, ntp - 1)),
-        ],
+        in_specs=[anywhere] * 12,
+        out_specs=(pl.BlockSpec(memory_space=pltpu.VMEM),) * 2,
+        scratch_shapes=scratch,
         compiler_params=pltpu.CompilerParams(
-            collective_id=0, has_side_effects=True, vmem_limit_bytes=60 * 1024 * 1024
+            collective_id=0, has_side_effects=True, vmem_limit_bytes=limit
         ),
     )(
         inputs.reshape(nz, INNER, rows, depth),

time: 40.9 us -> 36.8 us (0.90)
  local copies, waits for them, and re-layouts: 4.61 us -> 1.95 us
  Pallas kernels: 35.4 us -> 34.1 us
    unnamed x2, local copies, waits for them, and re-layouts: 4.61 us -> 1.95 us
    pallas_call x1, Pallas kernels: 35.4 us -> 34.1 us  [body(): pl.pallas_call(functools.partial(kernel, nkv, ntp), out_shape=(pltpu.VMEM...]
where the time goes in v3:
time: 36.8 us; the launch traced here: 36.6 us
  Pallas kernels  34.1 us (93%)
  local copies, waits for them, and re-layouts  1.95 us (5%)
  between operations  0.64 us (2%)
    pallas_call x1, Pallas kernels, body(): pl.pallas_call(functools.partial(kernel, nkv, ntp), out_shape=(pltpu.VMEM...  34.1 us
    unnamed x2, local copies, waits for them, and re-layouts  1.95 us

profile of v3, /device:TPU:0, one launch (start us, length us, event | category | flops | bytes accessed | tf_op | source)
XLA Modules:
  0.0 36.6 jit_solution(11725752517571807994)
XLA Ops:
  0.6 34.1 %shard_map.131 = (bf16[4,2,32,128]{3,2,1,0:T(8,128)(2,1)S(1)}, f32[8,4,128,128]{3,2,1,0:T(8,128)S(1)}) custom-call(bf16[4,2,32,512]{3,2,1,0:T(8,128)(2,1)} %bitcast.5, bf16[512]{0:T(512)(128)(2,1)} %gain_hbm.1, bf16[512,512]{1,0:T(8,128)(2,1)} %wq_hbm.1, bf16[512,512]{1,0:T(8,128)(2,1)} %wf_hbm.1, bf16[512,512]{1,0:T(8,128)(2,1)} %wv_hbm.1, ...), custom_call_target="tpu_custom_call" | custom-call | tf_op jit(solution)/shard_map/pallas_call | solution.py:393
  34.7 0.6 %copy.16 = bf16[256,128]{1,0:T(8,128)(2,1)} copy(bf16[256,128]{1,0:T(8,128)(2,1)S(1)} %bitcast.4) | data formatting | bytes 131072
  35.3 1.3 %copy.17 = f32[8,4,128,128]{3,2,1,0:T(8,128)} copy(f32[8,4,128,128]{3,2,1,0:T(8,128)S(1)} %get-tuple-element.7) | data formatting | bytes 4194304
